TPU v7x, 32 devices: a whole 2x2x4 slice. The times are simulated.
32 devices in a mesh: ep: 16 (over z, y, x), tp: 2 (over core).
Axes of the slice: x: 2, y: 2, z: 4, core: 2. Of those that a mesh axis runs over, the one named last changes fastest.
Arguments:
- hidden: bfloat16 [256, 2048], P('ep'), may hold values from -6 to 6
- attn_gain: bfloat16 [2048], replicated, may hold values from 0.099609375 to 1.8984375
- query_weight: bfloat16 [2048, 2048], P(None, 'tp'), may hold values from -0.125 to 0.125
- key_weight: bfloat16 [2048, 128], P(None, 'tp'), may hold values from -0.125 to 0.125
- value_weight: bfloat16 [2048, 128], P(None, 'tp'), may hold values from -0.125 to 0.125
- forget_weight: bfloat16 [2048, 32], P(None, 'tp'), may hold values from -0.125 to 0.125
- forget_bias: float32 [32], P('tp'), may hold values from -1 to 4
- cache_keys: bfloat16 [256, 2, 64, 1024], P('ep', 'tp'), may hold values from -64 to 64
- cache_values: bfloat16 [256, 2, 64, 1024], P('ep', 'tp'), may hold values from -6 to 6
- cache_logsum: float32 [256, 32, 1024], P('ep', 'tp'), may hold values from -144 to 0, as said below
- lengths: int32 [256], P('ep'), may hold values from 2 to 1023, as said below
- out_weight: bfloat16 [2048, 2048], P('ep'), may hold values from -0.125 to 0.125
- ffn_gain: bfloat16 [2048], replicated, may hold values from 0.099609375 to 1.8984375
- expert_ids: int32 [256, 6], P('ep'), may hold values from 0 to 15, all different within a row; in each aligned block of 16 rows (0 to 15, 16 to 31, ...) at most 12 rows name the same one
- expert_scores: float32 [256, 6], P('ep'), may hold values from 0.1 to 1
- gate_weights: bfloat16 [16, 2048, 512], P('ep', None, 'tp'), may hold values from -0.125 to 0.125
- up_weights: bfloat16 [16, 2048, 512], P('ep', None, 'tp'), may hold values from -0.125 to 0.125
- down_weights: bfloat16 [16, 512, 2048], P('ep', 'tp'), may hold values from -0.25 to 0.25
Outputs:
- updated: bfloat16 [256, 2048], P('ep')
- new_key: bfloat16 [256, 2, 64], P('ep', 'tp')
- new_value: bfloat16 [256, 2, 64], P('ep', 'tp')
- new_logsum: float32 [256, 32], P('ep', 'tp')
Inputs may be any that keep to these rules, and one draw needn't show every extreme that they name: `cache_logsum`: non-increasing along the positions. The new token stands at position lengths; some sequence has 1023 cached positions. `expert_ids`: each row names 6 different experts; the rows of one index of ep name one expert at most 12 times.
All inputs are finite; a program needn't handle non-finite values.
Results may differ from a plain program's by a relative error of at most 0.006.
Values may be sent and summed in bfloat16 or wider, within the bound.
A program may use at most 64 MiB of HBM per device.

v0:
```python
import jax
import jax.numpy as jnp
from jax import lax
from jax.sharding import PartitionSpec as P

HD = 64
TOP_K = 6
epsilon = 1e-06


def root_norm(values_in, gain):
    floats = values_in.astype(jnp.float32)
    inv_root = lax.rsqrt(jnp.mean(floats * floats, axis=-1, keepdims=True) + epsilon)
    return floats * inv_root * gain.astype(jnp.float32)


def per_device(
    hidden,
    attn_gain,
    query_weight,
    key_weight,
    value_weight,
    forget_weight,
    forget_bias,
    cache_keys,
    cache_values,
    cache_logsum,
    lengths,
    out_weight,
    ffn_gain,
    expert_ids,
    expert_scores,
    gate_weights,
    up_weights,
    down_weights,
):
    rows_here = hidden.shape[0]
    query_heads = query_weight.shape[1] // HD
    key_heads = key_weight.shape[1] // HD
    group_size = query_heads // key_heads
    cache_len = cache_keys.shape[-1]
    score_scale = HD ** (-0.5)
    normed = root_norm(hidden, attn_gain).astype(jnp.bfloat16)
    queries = jnp.dot(normed, query_weight, preferred_element_type=jnp.float32).astype(jnp.bfloat16)
    key_new = (
        jnp.dot(normed, key_weight, preferred_element_type=jnp.float32)
        .astype(jnp.bfloat16)
        .reshape(rows_here, key_heads, HD)
    )
    value_new = (
        jnp.dot(normed, value_weight, preferred_element_type=jnp.float32)
        .astype(jnp.bfloat16)
        .reshape(rows_here, key_heads, HD)
    )
    log_forget = jax.nn.log_sigmoid(
        jnp.dot(normed, forget_weight, preferred_element_type=jnp.float32) + forget_bias
    )
    positions = jnp.arange(cache_len, dtype=jnp.int32)
    is_last = positions[None, :] == (lengths - 1)[:, None]
    new_logsum = jnp.sum(jnp.where(is_last[:, None, :], cache_logsum, 0.0), axis=-1) + log_forget
    grouped = queries.reshape(rows_here, key_heads, group_size, HD)
    scores = jnp.einsum("sgjd,sgdp->sgjp", grouped, cache_keys, preferred_element_type=jnp.float32)
    scores = scores.reshape(rows_here, query_heads, cache_len) * score_scale
    scores = scores + new_logsum[:, :, None] - cache_logsum
    is_live = positions[None, :] < lengths[:, None]
    scores = jnp.where(is_live[:, None, :], scores, -jnp.inf)
    own_score = (
        jnp.einsum("sgjd,sgd->sgj", grouped, key_new, preferred_element_type=jnp.float32).reshape(
            rows_here, query_heads
        )
        * score_scale
    )
    top_score = jnp.maximum(jnp.max(scores, axis=-1), own_score)
    past_exp = jnp.exp(scores - top_score[:, :, None])
    own_exp = jnp.exp(own_score - top_score)
    denominator = jnp.sum(past_exp, axis=-1) + own_exp
    past_weight = (past_exp / denominator[:, :, None]).astype(jnp.bfloat16)
    own_weight = (own_exp / denominator).astype(jnp.bfloat16)
    attended = jnp.einsum(
        "sgjp,sgdp->sgjd",
        past_weight.reshape(rows_here, key_heads, group_size, cache_len),
        cache_values,
        preferred_element_type=jnp.float32,
    )
    attended = (
        attended
        + own_weight.astype(jnp.float32).reshape(rows_here, key_heads, group_size)[:, :, :, None]
        * value_new.astype(jnp.float32)[:, :, None, :]
    )
    attended = attended.reshape(rows_here, query_heads * HD).astype(jnp.bfloat16)
    whole_heads = lax.all_gather(attended, "tp", axis=1, tiled=True)
    projected = lax.dot_general(
        lax.all_gather(whole_heads, "ep", axis=0, tiled=True),
        out_weight,
        (((1,), (1,)), ((), ())),
        preferred_element_type=jnp.float32,
    ).astype(jnp.bfloat16)
    mixed = lax.all_to_all(projected, "ep", split_axis=0, concat_axis=1, tiled=True)
    residual = hidden.astype(jnp.float32) + mixed.astype(jnp.float32)
    ffn_in = root_norm(residual, ffn_gain).astype(jnp.bfloat16)
    ep_size = lax.axis_size("ep")
    local_experts = gate_weights.shape[0]
    experts = ep_size * local_experts
    route_count = rows_here * TOP_K
    capacity = 2 * ((route_count + experts - 1) // experts)
    flat_ids = expert_ids.reshape(route_count)
    onehot = (flat_ids[:, None] == jnp.arange(experts, dtype=jnp.int32)[None, :]).astype(jnp.int32)
    running = jnp.cumsum(onehot, axis=0)
    slot_index = jnp.sum(running * onehot, axis=1) - 1
    target = flat_ids * capacity + slot_index
    dispatch_map = (
        target[:, None] == jnp.arange(experts * capacity, dtype=jnp.int32)[None, :]
    ).astype(jnp.bfloat16)
    route_rows = jnp.repeat(ffn_in, TOP_K, axis=0)
    outgoing = lax.dot_general(
        dispatch_map, route_rows, (((0,), (0,)), ((), ())), preferred_element_type=jnp.float32
    )
    outgoing = outgoing.astype(jnp.bfloat16).reshape(
        ep_size, local_experts, capacity, ffn_in.shape[1]
    )
    arrived = lax.all_to_all(outgoing, "ep", split_axis=0, concat_axis=0, tiled=True)
    gate_act = jnp.einsum(
        "sekd,edf->sekf", arrived, gate_weights, preferred_element_type=jnp.float32
    )
    up_act = jnp.einsum("sekd,edf->sekf", arrived, up_weights, preferred_element_type=jnp.float32)
    hidden_act = (jax.nn.silu(gate_act) * up_act).astype(jnp.bfloat16)
    partial_out = jnp.einsum(
        "sekf,efd->sekd", hidden_act, down_weights, preferred_element_type=jnp.float32
    )
    half_sum = lax.psum_scatter(
        partial_out.astype(jnp.bfloat16), "tp", scatter_dimension=3, tiled=True
    )
    sent_back = lax.all_to_all(half_sum, "ep", split_axis=0, concat_axis=0, tiled=True)
    share_width = sent_back.shape[-1]
    picked = jnp.dot(
        dispatch_map,
        sent_back.reshape(experts * capacity, share_width),
        preferred_element_type=jnp.float32,
    )
    route_weight = expert_scores / jnp.sum(expert_scores, axis=-1, keepdims=True)
    expert_mix = jnp.sum(
        picked.reshape(rows_here, TOP_K, share_width) * route_weight[:, :, None], axis=1
    )
    own_part = lax.dynamic_slice_in_dim(
        residual, lax.axis_index("tp") * share_width, share_width, 1
    )
    updated = lax.all_gather((own_part + expert_mix).astype(jnp.bfloat16), "tp", axis=1, tiled=True)
    return (updated, key_new, value_new, new_logsum)


def solution(mesh):
    in_specs = (
        P("ep", None),
        P(),
        P(None, "tp"),
        P(None, "tp"),
        P(None, "tp"),
        P(None, "tp"),
        P("tp"),
        P("ep", "tp", None, None),
        P("ep", "tp", None, None),
        P("ep", "tp", None),
        P("ep"),
        P("ep", None),
        P(),
        P("ep", None),
        P("ep", None),
        P("ep", None, "tp"),
        P("ep", None, "tp"),
        P("ep", "tp", None),
    )
    out_specs = (P("ep", None), P("ep", "tp", None), P("ep", "tp", None), P("ep", "tp"))
    return jax.shard_map(
        per_device, mesh=mesh, in_specs=in_specs, out_specs=out_specs, check_vma=False
    )
```

profile of v0, /device:TPU:0, one launch (start us, length us, event | category | flops | bytes accessed | tf_op | source)
XLA Modules:
  0.0 167.7 jit_solution(6196648160617285266)
XLA Ops:
  7.2 0.0 copy-start
  7.2 0.0 all-gather.2.cloned.1.call-start
  7.2 0.8 broadcast_add_fusion.1
  8.0 0.7 iota_compare_fusion.4
  8.8 0.7 convert_element_type.86
  9.5 1.0 fusion.48
  10.4 0.0 copy-start.1
  10.5 0.0 copy-start.13
  10.5 0.0 copy-start.14
  10.5 3.0 %convolution_convert_fusion.3 = bf16[16,1024]{1,0:T(8,128)(2,1)S(1)} fusion(bf16[2048,1024]{1,0:T(8,128)(2,1)} %param.20, bf16[16,2048]{1,0:T(8,128)(2,1)} %param.18, f32[2048]{0:T(1024)S(1)} %convert_element_type.86, f32[16]{0:T(128)S(1)} %add_rsqrt_fusion.1), kind=kOutput, calls=%fused_computation.21 | convolution fusion | flops 67256320 | bytes 4300864 | tf_op jit(solution)/shard_map/dot_general | solution.py:44
  13.5 0.1 reshape.203
  13.6 0.1 iota_compare_fusion.3
  13.7 1.2 convolution_convert_fusion.5
  14.9 0.2 select_reduce_fusion
  15.1 0.1 fusion.59
  15.2 0.2 fusion.58
  15.5 0.0 copy-done
  15.5 0.0 copy-start.8
  15.5 0.0 copy-start.5
  15.5 0.0 copy-start.10
  15.5 0.5 fusion.68
  16.1 0.0 copy-done.8
  16.1 0.3 fusion.31
  16.4 0.0 copy-done.5
  16.5 0.8 fusion.69
  17.3 0.0 copy-done.10
  17.3 0.7 fusion.23
  18.0 0.1 convert_element_type.96
  18.2 2.1 %all_gather.9 = bf16[16,2048]{1,0:T(8,128)(2,1)} all-gather(bf16[16,1024]{1,0:T(8,128)(2,1)S(1)} %convert_element_type.96), channel_id=1, replica_groups=mesh['ep'=16,'tp'=2] {'tp'}, dimensions={1}, use_global_device_ids=true | all-gather | bytes 98304 | tf_op jit(solution)/shard_map/all_gather | solution.py:91
  20.3 0.0 all-gather.2.cloned.1.call-update
  20.3 0.0 copy-done.9
  20.3 0.1 copy.41
  20.4 0.1 eq.67
  20.5 0.1 fusion.56
  20.6 0.1 reduce_window_sum.11
  20.7 0.2 select_reduce_fusion.1
  20.9 57.2 %all-gather.2.cloned.1.call-done = bf16[256,2048]{1,0:T(8,128)(2,1)} async-done(((bf16[16,2048]{1,0:T(8,128)(2,1)}), bf16[256,2048]{1,0:T(8,128)(2,1)}) %all-gather.2.cloned.1.call-update) | async-done | bytes 1048592 | tf_op jit(solution)/shard_map/all_gather | solution.py:93
  78.1 2.3 %convolution_convert_fusion.2 = bf16[256,128]{1,0:T(8,128)(2,1)} fusion(bf16[256,2048]{1,0:T(8,128)(2,1)} %all-gather.2.cloned.1.call-done, bf16[128,2048]{1,0:T(8,128)(2,1)S(1)} %copy-done.4), kind=kOutput, calls=%fused_computation.20 | convolution fusion | flops 134250496 | bytes 1638400 | tf_op jit(solution)/shard_map/dot_general | solution.py:92
  80.4 4.5 %all-to-all-start = ((bf16[16,16,128]{2,1,0:T(8,128)(2,1)}), bf16[16,16,128]{2,1,0:T(8,128)(2,1)S(1)}, u32[]{:S(2)}, u32[]{:S(2)}) async-start(bf16[16,16,128]{2,1,0:T(8,128)(2,1)} %bitcast.5), calls=%async_computation | async-start | bytes 131072 | tf_op jit(solution)/shard_map/all_to_all | solution.py:98
  84.9 0.0 reduce-scatter.2.cloned.1.call-start
  85.0 7.5 %all-to-all-done = bf16[16,16,128]{2,1,0:T(8,128)(2,1)S(1)} async-done(((bf16[16,16,128]{2,1,0:T(8,128)(2,1)}), bf16[16,16,128]{2,1,0:T(8,128)(2,1)S(1)}, u32[]{:S(2)}, u32[]{:S(2)}) %all-to-all-start) | async-done | bytes 65568 | tf_op jit(solution)/shard_map/all_to_all | solution.py:98
  92.4 0.1 multiply_reduce_fusion
  92.6 0.1 multiply_convert_fusion
  92.7 0.1 broadcast_in_dim.26
  92.7 0.1 reshape.206
  92.9 1.4 convolution_convert_fusion.1
  94.2 1.3 reshape.207
  95.5 0.0 copy-start.11
  95.5 25.9 %all_to_all.23 = bf16[16,1,12,2048]{3,2,1,0:T(8,128)(2,1)S(1)} all-to-all(bf16[16,1,12,2048]{3,2,1,0:T(8,128)(2,1)S(1)} %bitcast.98), channel_id=1, replica_groups=mesh['ep'=16,'tp'=2] {'ep'}, dimensions={0} | all-to-all | bytes 1572864 | tf_op jit(solution)/shard_map/all_to_all | solution.py:121
  121.4 1.0 copy-done.3
  122.4 0.6 convolution_bitcast_fusion.1
  123.0 0.6 copy-done.12
  123.6 3.5 %fusion = bf16[16,1,12,2048]{3,0,2,1:T(8,128)(2,1)} fusion(bf16[1,256,2048]{2,1,0:T(8,128)(2,1)S(1)} %copy-done.12, bf16[1,2048,256]{2,1,0:T(8,128)(2,1)} %param.34, bf16[16,1,12,2048]{3,2,1,0:T(8,128)(2,1)} %copy-done.3, f32[16,1,12,256]{3,0,2,1:T(8,128)S(1)} %convolution_bitcast_fusion.1), kind=kOutput, calls=%fused_computation.2 | convolution fusion | flops 403341312 | bytes 3866624 | tf_op jit(solution)/shard_map/sekf,efd->sekd/dot_general | solution.py:127
  127.1 0.0 reduce-scatter.2.cloned.1.call-update
  127.2 6.6 %reduce-scatter.2.cloned.1.call-done = bf16[16,1,12,1024]{3,0,2,1:T(8,128)(2,1)} async-done(((bf16[16,1,12,2048]{3,0,2,1:T(8,128)(2,1)}), bf16[16,1,12,1024]{3,0,2,1:T(8,128)(2,1)}) %reduce-scatter.2.cloned.1.call-update) | async-done | bytes 393232 | tf_op jit(solution)/shard_map/reduce_scatter | solution.py:130
  133.7 2.0 %copy.45 = bf16[16,1,12,1024]{3,2,1,0:T(8,128)(2,1)} copy(bf16[16,1,12,1024]{3,0,2,1:T(8,128)(2,1)} %reduce-scatter.2.cloned.1.call-done) | data formatting | bytes 786432 | tf_op jit(solution)/shard_map/reduce_scatter | solution.py:130
  135.7 6.7 %all-to-all-start.2 = ((bf16[16,1,12,1024]{3,2,1,0:T(8,128)(2,1)}), bf16[16,1,12,1024]{3,2,1,0:T(8,128)(2,1)S(1)}, u32[]{:S(2)}, u32[]{:S(2)}) async-start(bf16[16,1,12,1024]{3,2,1,0:T(8,128)(2,1)} %copy.45), calls=%async_computation.3 | async-start | bytes 1048576 | tf_op jit(solution)/shard_map/all_to_all | solution.py:133
  142.5 0.1 sub.33
  142.5 0.1 copy.42
  142.7 15.3 %all-to-all-done.2 = bf16[16,1,12,1024]{3,2,1,0:T(8,128)(2,1)S(1)} async-done(((bf16[16,1,12,1024]{3,2,1,0:T(8,128)(2,1)}), bf16[16,1,12,1024]{3,2,1,0:T(8,128)(2,1)S(1)}, u32[]{:S(2)}, u32[]{:S(2)}) %all-to-all-start.2) | async-done | bytes 393248 | tf_op jit(solution)/shard_map/all_to_all | solution.py:133
  158.0 0.1 reshape.222
  158.0 0.3 fusion.17
  158.3 1.9 %all_gather.11 = bf16[16,2048]{1,0:T(8,128)(2,1)S(1)} all-gather(bf16[16,1024]{1,0:T(8,128)(2,1)S(1)} %add_convert_fusion), channel_id=1, replica_groups=mesh['ep'=16,'tp'=2] {'tp'}, dimensions={1}, use_global_device_ids=true | all-gather | bytes 98304 | tf_op jit(solution)/shard_map/all_gather | solution.py:147
  160.2 0.6 copy.63
  (27 shorter events, 0.1 us)
Async XLA Ops:
  7.2 8.3 %copy-start = (bf16[16,1,64,1024]{3,2,1,0:T(8,128)(2,1)S(1)}, bf16[16,1,64,1024]{3,2,1,0:T(8,128)(2,1)}, u32[]{:S(2)}) copy-start(bf16[16,1,64,1024]{3,2,1,0:T(8,128)(2,1)} %param.25) | copy-start | bytes 6291460
  7.2 71.0 %all-gather.2.cloned.1.call-start = ((), (), s32[]{:S(2)}) async-start(), calls=%async_computation.4 | async-start | bytes 1114112 | tf_op jit(solution)/shard_map/all_gather | solution.py:93
  10.4 3.3 %copy-start.2 = (bf16[16,2048]{1,0:T(8,128)(2,1)S(1)}, bf16[16,2048]{1,0:T(8,128)(2,1)}, u32[]{:S(2)}) copy-start(bf16[16,2048]{1,0:T(8,128)(2,1)} %param.18) | copy-start | bytes 196612
  10.4 4.4 %copy-start.1 = (f32[16,16,1024]{2,1,0:T(8,128)S(1)}, f32[16,16,1024]{2,1,0:T(8,128)}, u32[]{:S(2)}) copy-start(f32[16,16,1024]{2,1,0:T(8,128)} %param.27) | copy-start | bytes 3145732
  10.5 4.8 %copy-start.13 = (bf16[2048,16]{0,1:T(8,128)(2,1)S(1)}, bf16[2048,16]{0,1:T(8,128)(2,1)}, u32[]{:S(2)}) copy-start(bf16[2048,16]{0,1:T(8,128)(2,1)} %param.23) | copy-start | bytes 196612
  10.5 4.8 %copy-start.14 = (f32[16]{0:T(128)S(1)}, f32[16]{0:T(128)}, u32[]{:S(2)}) copy-start(f32[16]{0:T(128)} %param.24) | copy-start | bytes 196
  14.9 1.2 copy-start.15
  15.5 0.6 copy-start.8
  15.5 1.0 copy-start.5
  15.5 1.8 %copy-start.10 = (bf16[16,1,64,1024]{3,2,1,0:T(8,128)(2,1)S(1)}, bf16[16,1,64,1024]{3,2,1,0:T(8,128)(2,1)}, u32[]{:S(2)}) copy-start(bf16[16,1,64,1024]{3,2,1,0:T(8,128)(2,1)} %param.26) | copy-start | bytes 6291460
  17.3 3.0 %copy-start.9 = (bf16[2048]{0:T(1024)(128)(2,1)S(1)}, bf16[2048]{0:T(1024)(128)(2,1)}, u32[]{:S(2)}) copy-start(bf16[2048]{0:T(1024)(128)(2,1)} %param.30) | copy-start | bytes 12292
  17.3 3.0 %copy-start.6 = (s32[16,6]{0,1:T(8,128)S(1)}, s32[16,6]{0,1:T(8,128)}, u32[]{:S(2)}) copy-start(s32[16,6]{0,1:T(8,128)} %param.31) | copy-start | bytes 1156
  17.3 60.8 %copy-start.4 = (bf16[128,2048]{1,0:T(8,128)(2,1)S(1)}, bf16[128,2048]{1,0:T(8,128)(2,1)}, u32[]{:S(2)}) copy-start(bf16[128,2048]{1,0:T(8,128)(2,1)} %param.29) | copy-start | bytes 1572868
  80.4 12.0 %all-to-all-start = ((bf16[16,16,128]{2,1,0:T(8,128)(2,1)}), bf16[16,16,128]{2,1,0:T(8,128)(2,1)S(1)}, u32[]{:S(2)}, u32[]{:S(2)}) async-start(bf16[16,16,128]{2,1,0:T(8,128)(2,1)} %bitcast.5), calls=%async_computation | async-start | bytes 131072 | tf_op jit(solution)/shard_map/all_to_all | solution.py:98
  84.9 48.8 %reduce-scatter.2.cloned.1.call-start = ((), (), s32[]{:S(2)}) async-start(), calls=%async_computation.5 | async-start | bytes 1179648 | tf_op jit(solution)/shard_map/reduce_scatter | solution.py:130
  95.5 26.9 %copy-start.11 = (bf16[1,2048,256]{2,1,0:T(8,128)(2,1)S(1)}, bf16[1,2048,256]{2,1,0:T(8,128)(2,1)}, u32[]{:S(2)}) copy-start(bf16[1,2048,256]{2,1,0:T(8,128)(2,1)} %param.33) | copy-start | bytes 3145732
  121.4 1.0 copy-start.3
  122.4 1.2 copy-start.12
  127.1 15.5 %copy-start.7 = (f32[16,6]{0,1:T(8,128)S(1)}, f32[16,6]{0,1:T(8,128)}, u32[]{:S(2)}) copy-start(f32[16,6]{0,1:T(8,128)} %param.32) | copy-start | bytes 1156
  135.7 22.2 %all-to-all-start.2 = ((bf16[16,1,12,1024]{3,2,1,0:T(8,128)(2,1)}), bf16[16,1,12,1024]{3,2,1,0:T(8,128)(2,1)S(1)}, u32[]{:S(2)}, u32[]{:S(2)}) async-start(bf16[16,1,12,1024]{3,2,1,0:T(8,128)(2,1)} %copy.45), calls=%async_computation.3 | async-start | bytes 1048576 | tf_op jit(solution)/shard_map/all_to_all | solution.py:133
Sparse Core Ops, SparseCore 0:
  20.4 57.6 all-gather.1
  127.3 6.3 reduce-scatter.1
where the time goes:
time: 168 us
  waiting for transfers between devices  86.5 us (51%)
  blocking collectives  29.9 us (18%)
  matrix products  14.7 us (9%)
  between operations  14.3 us (9%)
  starting transfers between devices  11.3 us (7%)
  local copies, waits for them, and re-layouts  6.49 us (4%)
  other arithmetic  4.48 us (3%)
    all_gather x1, waiting for transfers between devices, per_device(): lax.all_gather(whole_heads, 'ep', axis=0, tiled=True)  57.2 us
    all_to_all x1, blocking collectives, per_device(): lax.all_to_all(outgoing, 'ep', split_axis=0, concat_axis=0, tiled=True)  25.9 us
    all_to_all x1, waiting for transfers between devices, per_device(): lax.all_to_all(half_sum, 'ep', split_axis=0, concat_axis=0, tiled=True)  15.3 us
    all_to_all x1, waiting for transfers between devices, per_device(): lax.all_to_all(projected, 'ep', split_axis=0, concat_axis=1, tiled=True)  7.47 us
    all_to_all x1, starting transfers between devices, per_device(): lax.all_to_all(half_sum, 'ep', split_axis=0, concat_axis=0, tiled=True)  6.74 us
    reduce_scatter x1, waiting for transfers between devices, per_device(): lax.psum_scatter(partial_out.astype(jnp.bfloat16), 'tp', scatter_dimensio...  6.55 us
    all_to_all x1, starting transfers between devices, per_device(): lax.all_to_all(projected, 'ep', split_axis=0, concat_axis=1, tiled=True)  4.46 us
    dot_general x1, matrix products, per_device(): jnp.einsum('sekf,efd->sekd', hidden_act, down_weights, preferred_element_...  3.53 us
  transfers between devices with their start and end apart: 4, of which 4 were waited for; matrix products, arithmetic and copies ran while one was open for 0% of the time, Pallas kernels for 0%

commit v1 on v0

--- a/solution.py
+++ b/solution.py
@@ -95,7 +95,10 @@
         (((1,), (1,)), ((), ())),
         preferred_element_type=jnp.float32,
     ).astype(jnp.bfloat16)
-    mixed = lax.all_to_all(projected, "ep", split_axis=0, concat_axis=1, tiled=True)
+    mixed = jnp.concatenate(
+        lax.all_to_all(jnp.stack(jnp.split(projected, lax.axis_size("ep"), axis=0)), "ep", 0, 0),
+        axis=1,
+    )
     residual = hidden.astype(jnp.float32) + mixed.astype(jnp.float32)
     ffn_in = root_norm(residual, ffn_gain).astype(jnp.bfloat16)
     ep_size = lax.axis_size("ep")

time: 168 us -> 177 us (1.054)
  local copies, waits for them, and re-layouts: 6.49 us -> 16 us
    unnamed x34 -> x49, local copies, waits for them, and re-layouts: 2.45 us -> 11.3 us
where the time goes in v1:
time: 177 us
  waiting for transfers between devices  86.5 us (49%)
  blocking collectives  29.9 us (17%)
  local copies, waits for them, and re-layouts  16 us (9%)
  between operations  14.4 us (8%)
  matrix products  14 us (8%)
  starting transfers between devices  11.3 us (6%)
  other arithmetic  4.48 us (3%)
    all_gather x1, waiting for transfers between devices, per_device(): lax.all_gather(whole_heads, 'ep', axis=0, tiled=True)  57.2 us
    all_to_all x1, blocking collectives, per_device(): lax.all_to_all(outgoing, 'ep', split_axis=0, concat_axis=0, tiled=True)  25.9 us
    all_to_all x1, waiting for transfers between devices, per_device(): lax.all_to_all(half_sum, 'ep', split_axis=0, concat_axis=0, tiled=True)  15.3 us
    unnamed x49, local copies, waits for them, and re-layouts  11.3 us
    all_to_all x1, waiting for transfers between devices, per_device(): lax.all_to_all(jnp.stack(jnp.split(projected, lax.axis_size('ep'), axis=0...  7.47 us
    all_to_all x1, starting transfers between devices, per_device(): lax.all_to_all(half_sum, 'ep', split_axis=0, concat_axis=0, tiled=True)  6.74 us
    reduce_scatter x1, waiting for transfers between devices, per_device(): lax.psum_scatter(partial_out.astype(jnp.bfloat16), 'tp', scatter_dimensio...  6.55 us
    all_to_all x1, starting transfers between devices, per_device(): lax.all_to_all(jnp.stack(jnp.split(projected, lax.axis_size('ep'), axis=0...  4.46 us
  transfers between devices with their start and end apart: 4, of which 4 were waited for; matrix products, arithmetic and copies ran while one was open for 0% of the time, Pallas kernels for 0%

profile of v1, /device:TPU:0, one launch (start us, length us, event | category | flops | bytes accessed | tf_op | source)
XLA Modules:
  0.0 176.5 jit_solution(2353030339799074804)
XLA Ops:
  7.2 0.8 broadcast_add_fusion.1
  8.0 0.7 iota_compare_fusion.4
  8.8 0.7 convert_element_type.86
  9.5 1.0 fusion.48
  10.5 3.0 %convolution_convert_fusion.3 = bf16[16,1024]{1,0:T(8,128)(2,1)S(1)} fusion(bf16[2048,1024]{1,0:T(8,128)(2,1)} %param.20, bf16[16,2048]{1,0:T(8,128)(2,1)} %param.18, f32[2048]{0:T(1024)S(1)} %convert_element_type.86, f32[16]{0:T(128)S(1)} %add_rsqrt_fusion.1), kind=kOutput, calls=%fused_computation.21 | convolution fusion | flops 67256320 | bytes 4300864 | tf_op jit(solution)/shard_map/dot_general | solution.py:44
  13.5 0.1 reshape.202
  13.6 0.1 iota_compare_fusion.3
  13.7 1.2 convolution_convert_fusion.5
  14.9 0.2 select_reduce_fusion
  15.1 0.1 fusion.59
  15.2 0.2 fusion.58
  15.5 0.5 fusion.68
  16.1 0.0 copy-done.8
  16.1 0.3 fusion.31
  16.5 0.8 fusion.69
  17.3 0.7 fusion.23
  18.0 0.1 convert_element_type.96
  18.2 2.1 %all_gather.9 = bf16[16,2048]{1,0:T(8,128)(2,1)} all-gather(bf16[16,1024]{1,0:T(8,128)(2,1)S(1)} %convert_element_type.96), channel_id=1, replica_groups=mesh['ep'=16,'tp'=2] {'tp'}, dimensions={1}, use_global_device_ids=true | all-gather | bytes 98304 | tf_op jit(solution)/shard_map/all_gather | solution.py:91
  20.3 0.1 copy.40
  20.4 0.1 eq.67
  20.5 0.1 fusion.56
  20.6 0.1 reduce_window_sum.11
  20.7 0.2 select_reduce_fusion.1
  20.9 57.2 %all-gather.2.cloned.1.call-done = bf16[256,2048]{1,0:T(8,128)(2,1)} async-done(((bf16[16,2048]{1,0:T(8,128)(2,1)}), bf16[256,2048]{1,0:T(8,128)(2,1)}) %all-gather.2.cloned.1.call-update) | async-done | bytes 1048592 | tf_op jit(solution)/shard_map/all_gather | solution.py:93
  78.1 1.7 convolution_convert_fusion.2
  79.8 0.6 constant_dynamic-update-slice_fusion.15
  80.4 0.6 constant_dynamic-update-slice_fusion.14
  81.0 0.6 constant_dynamic-update-slice_fusion.13
  81.6 0.6 constant_dynamic-update-slice_fusion.12
  82.2 0.6 constant_dynamic-update-slice_fusion.11
  82.8 0.6 constant_dynamic-update-slice_fusion.10
  83.4 0.6 constant_dynamic-update-slice_fusion.9
  84.0 0.6 constant_dynamic-update-slice_fusion.8
  84.6 0.6 constant_dynamic-update-slice_fusion.7
  85.1 0.6 constant_dynamic-update-slice_fusion.6
  85.7 0.6 constant_dynamic-update-slice_fusion.5
  86.3 0.6 constant_dynamic-update-slice_fusion.4
  86.9 0.6 constant_dynamic-update-slice_fusion.3
  87.5 0.6 constant_dynamic-update-slice_fusion.2
  88.1 0.6 constant_dynamic-update-slice_fusion.1
  88.7 0.6 constant_dynamic-update-slice_fusion
  89.3 4.5 %all-to-all-start = ((bf16[16,16,128]{2,1,0:T(8,128)(2,1)}), bf16[16,16,128]{2,1,0:T(8,128)(2,1)S(1)}, u32[]{:S(2)}, u32[]{:S(2)}) async-start(bf16[16,16,128]{2,1,0:T(8,128)(2,1)} %constant_dynamic-update-slice_fusion), calls=%async_computation | async-start | bytes 131072 | tf_op jit(solution)/shard_map/all_to_all | solution.py:99
  93.8 7.5 %all-to-all-done = bf16[16,16,128]{2,1,0:T(8,128)(2,1)S(1)} async-done(((bf16[16,16,128]{2,1,0:T(8,128)(2,1)}), bf16[16,16,128]{2,1,0:T(8,128)(2,1)S(1)}, u32[]{:S(2)}, u32[]{:S(2)}) %all-to-all-start) | async-done | bytes 65568 | tf_op jit(solution)/shard_map/all_to_all | solution.py:99
  101.3 0.1 multiply_reduce_fusion
  101.5 0.1 multiply_convert_fusion
  101.5 0.1 broadcast_in_dim.26
  101.6 0.1 reshape.205
  101.8 1.4 convolution_convert_fusion.1
  103.1 1.3 reshape.206
  104.4 25.9 %all_to_all.15 = bf16[16,1,12,2048]{3,2,1,0:T(8,128)(2,1)S(1)} all-to-all(bf16[16,1,12,2048]{3,2,1,0:T(8,128)(2,1)S(1)} %bitcast.161), channel_id=1, replica_groups=mesh['ep'=16,'tp'=2] {'ep'}, dimensions={0} | all-to-all | bytes 1572864 | tf_op jit(solution)/shard_map/all_to_all | solution.py:124
  130.3 1.0 copy-done.3
  131.3 0.6 convolution_bitcast_fusion.1
  131.9 0.6 copy-done.12
  132.5 3.5 %fusion = bf16[16,1,12,2048]{3,0,2,1:T(8,128)(2,1)} fusion(bf16[1,256,2048]{2,1,0:T(8,128)(2,1)S(1)} %copy-done.12, bf16[1,2048,256]{2,1,0:T(8,128)(2,1)} %param.34, bf16[16,1,12,2048]{3,2,1,0:T(8,128)(2,1)} %copy-done.3, f32[16,1,12,256]{3,0,2,1:T(8,128)S(1)} %convolution_bitcast_fusion.1), kind=kOutput, calls=%fused_computation.2 | convolution fusion | flops 403341312 | bytes 3866624 | tf_op jit(solution)/shard_map/sekf,efd->sekd/dot_general | solution.py:130
  136.0 6.6 %reduce-scatter.2.cloned.1.call-done = bf16[16,1,12,1024]{3,0,2,1:T(8,128)(2,1)} async-done(((bf16[16,1,12,2048]{3,0,2,1:T(8,128)(2,1)}), bf16[16,1,12,1024]{3,0,2,1:T(8,128)(2,1)}) %reduce-scatter.2.cloned.1.call-update) | async-done | bytes 393232 | tf_op jit(solution)/shard_map/reduce_scatter | solution.py:133
  142.6 2.0 %copy.44 = bf16[16,1,12,1024]{3,2,1,0:T(8,128)(2,1)} copy(bf16[16,1,12,1024]{3,0,2,1:T(8,128)(2,1)} %reduce-scatter.2.cloned.1.call-done) | data formatting | bytes 786432 | tf_op jit(solution)/shard_map/reduce_scatter | solution.py:133
  144.6 6.7 %all-to-all-start.2 = ((bf16[16,1,12,1024]{3,2,1,0:T(8,128)(2,1)}), bf16[16,1,12,1024]{3,2,1,0:T(8,128)(2,1)S(1)}, u32[]{:S(2)}, u32[]{:S(2)}) async-start(bf16[16,1,12,1024]{3,2,1,0:T(8,128)(2,1)} %copy.44), calls=%async_computation.3 | async-start | bytes 1048576 | tf_op jit(solution)/shard_map/all_to_all | solution.py:136
  151.3 0.1 sub.33
  151.4 0.1 copy.41
  151.6 15.3 %all-to-all-done.2 = bf16[16,1,12,1024]{3,2,1,0:T(8,128)(2,1)S(1)} async-done(((bf16[16,1,12,1024]{3,2,1,0:T(8,128)(2,1)}), bf16[16,1,12,1024]{3,2,1,0:T(8,128)(2,1)S(1)}, u32[]{:S(2)}, u32[]{:S(2)}) %all-to-all-start.2) | async-done | bytes 393248 | tf_op jit(solution)/shard_map/all_to_all | solution.py:136
  166.8 0.1 reshape.221
  166.9 0.3 fusion.17
  167.2 1.9 %all_gather.11 = bf16[16,2048]{1,0:T(8,128)(2,1)S(1)} all-gather(bf16[16,1024]{1,0:T(8,128)(2,1)S(1)} %add_convert_fusion), channel_id=1, replica_groups=mesh['ep'=16,'tp'=2] {'tp'}, dimensions={1}, use_global_device_ids=true | all-gather | bytes 98304 | tf_op jit(solution)/shard_map/all_gather | solution.py:150
  169.1 0.6 copy.77
  (43 shorter events, 0.3 us)
Async XLA Ops:
  7.2 8.3 %copy-start = (bf16[16,1,64,1024]{3,2,1,0:T(8,128)(2,1)S(1)}, bf16[16,1,64,1024]{3,2,1,0:T(8,128)(2,1)}, u32[]{:S(2)}) copy-start(bf16[16,1,64,1024]{3,2,1,0:T(8,128)(2,1)} %param.25) | copy-start | bytes 6291460
  7.2 71.0 %all-gather.2.cloned.1.call-start = ((), (), s32[]{:S(2)}) async-start(), calls=%async_computation.4 | async-start | bytes 1114112 | tf_op jit(solution)/shard_map/all_gather | solution.py:93
  10.4 3.3 %copy-start.2 = (bf16[16,2048]{1,0:T(8,128)(2,1)S(1)}, bf16[16,2048]{1,0:T(8,128)(2,1)}, u32[]{:S(2)}) copy-start(bf16[16,2048]{1,0:T(8,128)(2,1)} %param.18) | copy-start | bytes 196612
  10.4 4.4 %copy-start.1 = (f32[16,16,1024]{2,1,0:T(8,128)S(1)}, f32[16,16,1024]{2,1,0:T(8,128)}, u32[]{:S(2)}) copy-start(f32[16,16,1024]{2,1,0:T(8,128)} %param.27) | copy-start | bytes 3145732
  10.5 4.8 %copy-start.13 = (bf16[2048,16]{0,1:T(8,128)(2,1)S(1)}, bf16[2048,16]{0,1:T(8,128)(2,1)}, u32[]{:S(2)}) copy-start(bf16[2048,16]{0,1:T(8,128)(2,1)} %param.23) | copy-start | bytes 196612
  10.5 4.8 %copy-start.14 = (f32[16]{0:T(128)S(1)}, f32[16]{0:T(128)}, u32[]{:S(2)}) copy-start(f32[16]{0:T(128)} %param.24) | copy-start | bytes 196
  14.9 1.2 copy-start.15
  15.5 0.6 copy-start.8
  15.5 1.0 copy-start.5
  15.5 1.8 %copy-start.10 = (bf16[16,1,64,1024]{3,2,1,0:T(8,128)(2,1)S(1)}, bf16[16,1,64,1024]{3,2,1,0:T(8,128)(2,1)}, u32[]{:S(2)}) copy-start(bf16[16,1,64,1024]{3,2,1,0:T(8,128)(2,1)} %param.26) | copy-start | bytes 6291460
  17.3 3.0 %copy-start.9 = (bf16[2048]{0:T(1024)(128)(2,1)S(1)}, bf16[2048]{0:T(1024)(128)(2,1)}, u32[]{:S(2)}) copy-start(bf16[2048]{0:T(1024)(128)(2,1)} %param.30) | copy-start | bytes 12292
  17.3 3.0 %copy-start.6 = (s32[16,6]{0,1:T(8,128)S(1)}, s32[16,6]{0,1:T(8,128)}, u32[]{:S(2)}) copy-start(s32[16,6]{0,1:T(8,128)} %param.31) | copy-start | bytes 1156
  17.3 60.8 %copy-start.4 = (bf16[128,2048]{1,0:T(8,128)(2,1)S(1)}, bf16[128,2048]{1,0:T(8,128)(2,1)}, u32[]{:S(2)}) copy-start(bf16[128,2048]{1,0:T(8,128)(2,1)} %param.29) | copy-start | bytes 1572868
  89.3 12.0 %all-to-all-start = ((bf16[16,16,128]{2,1,0:T(8,128)(2,1)}), bf16[16,16,128]{2,1,0:T(8,128)(2,1)S(1)}, u32[]{:S(2)}, u32[]{:S(2)}) async-start(bf16[16,16,128]{2,1,0:T(8,128)(2,1)} %constant_dynamic-update-slice_fusion), calls=%async_computation | async-start | bytes 131072 | tf_op jit(solution)/shard_map/all_to_all | solution.py:99
  93.8 48.8 %reduce-scatter.2.cloned.1.call-start = ((), (), s32[]{:S(2)}) async-start(), calls=%async_computation.5 | async-start | bytes 1179648 | tf_op jit(solution)/shard_map/reduce_scatter | solution.py:133
  104.4 26.9 %copy-start.11 = (bf16[1,2048,256]{2,1,0:T(8,128)(2,1)S(1)}, bf16[1,2048,256]{2,1,0:T(8,128)(2,1)}, u32[]{:S(2)}) copy-start(bf16[1,2048,256]{2,1,0:T(8,128)(2,1)} %param.33) | copy-start | bytes 3145732
  130.3 1.0 copy-start.3
  131.2 1.2 copy-start.12
  136.0 15.5 %copy-start.7 = (f32[16,6]{0,1:T(8,128)S(1)}, f32[16,6]{0,1:T(8,128)}, u32[]{:S(2)}) copy-start(f32[16,6]{0,1:T(8,128)} %param.32) | copy-start | bytes 1156
  144.6 22.2 %all-to-all-start.2 = ((bf16[16,1,12,1024]{3,2,1,0:T(8,128)(2,1)}), bf16[16,1,12,1024]{3,2,1,0:T(8,128)(2,1)S(1)}, u32[]{:S(2)}, u32[]{:S(2)}) async-start(bf16[16,1,12,1024]{3,2,1,0:T(8,128)(2,1)} %copy.44), calls=%async_computation.3 | async-start | bytes 1048576 | tf_op jit(solution)/shard_map/all_to_all | solution.py:136
Sparse Core Ops, SparseCore 0:
  20.4 57.6 all-gather.1
  136.2 6.3 reduce-scatter.1
